TPU v7x, 32 devices: a whole 2x2x4 slice. The times are simulated.
32 devices in a mesh: sp: 8 (over z, x), tp: 4 (over y, core).
Axes of the slice: x: 2, y: 2, z: 4, core: 2. Of those that a mesh axis runs over, the one named last changes fastest.
Arguments:
- latent: bfloat16 [6144, 2048], P(('sp', 'tp')), may hold values from -6 to 6
- context: bfloat16 [1024, 2048], P('sp'), may hold values from -6 to 6
- conditioning: float32 [2, 2048], replicated, may hold values from -6 to 6
- norm_gain: float32 [2048], replicated, may hold values from 0.1 to 1.9
- mod_shift: bfloat16 [2048, 2048], P('sp', 'tp'), may hold values from -0.1875 to 0.1875
- mod_scale: bfloat16 [2048, 2048], P('sp', 'tp'), may hold values from -0.1875 to 0.1875
- mod_gate: bfloat16 [2048, 2048], P('sp', 'tp'), may hold values from -0.1875 to 0.1875
- w_query: bfloat16 [2048, 2048], P(None, 'tp'), may hold values from -4 to 4
- w_key: bfloat16 [2048, 2048], P(None, 'tp'), may hold values from -0.125 to 0.125
- w_value: bfloat16 [2048, 2048], P(None, 'tp'), may hold values from -0.125 to 0.125
- w_out: bfloat16 [2048, 2048], P('tp'), may hold values from -0.125 to 0.125
- lambdas: float32 [16], P('tp'), may hold values from 0.3 to 0.8
- context_bias: float32 [16], P('tp'), may hold values from 0.8 to 2.2
- head_gain: float32 [128], replicated, may hold values from 0.1 to 1.9
Outputs:
- updated: bfloat16 [6144, 2048], P(('sp', 'tp'))
All inputs are finite; a program needn't handle non-finite values.
Results may differ from a plain program's by a relative error of at most 0.01.
The roundings to bfloat16 on the way count: a program that leaves them out, or rounds other values in their place, can miss the bound.
Values may be sent and summed in bfloat16 or wider, within the bound.
No kernel may reach another device: no remote copies, remote signals or barrier semaphores. Data moves between devices by JAX's collectives and lax.ppermute only.
A program may use at most 128 MiB of HBM per device.

v0:
```python
import jax
import jax.numpy as jnp
from jax import lax
from jax.sharding import PartitionSpec as P

EPS = 1e-06
NEGATIVE = -1e30


def modulated(inputs, norm_scale, offset_vec, scale_vec):
    rows_float = inputs.astype(jnp.float32)
    normal = rows_float * lax.rsqrt(jnp.mean(rows_float * rows_float, axis=-1, keepdims=True) + EPS)
    return (normal * norm_scale * (1.0 + scale_vec) + offset_vec).astype(jnp.bfloat16)


def block_size(length):
    for candidate in range(min(length, 1024), 0, -1):
        if length % candidate == 0:
            return candidate
    return length


def absorb(running, portion, context_flags, queries, bias_heads):
    head_count = queries.shape[1]
    head_dim = queries.shape[3]
    row_count = portion.shape[0]
    head_cols = head_count * 2 * head_dim
    key_rows = portion[:, :head_cols].reshape(row_count, head_count, 2, head_dim)
    value_rows = portion[:, head_cols:].reshape(row_count, head_count, 2 * head_dim)
    shifts = bias_heads[:, None, None] * context_flags[None, None, :]
    updated = []
    for which_map in range(2):
        previous, weight, accumulated = running[3 * which_map : 3 * which_map + 3]
        scores = (
            jnp.einsum(
                "qhd,khd->hqk",
                queries[:, :, which_map],
                key_rows[:, :, which_map],
                preferred_element_type=jnp.float32,
            )
            * head_dim ** (-0.5)
            + shifts
        )
        peak_new = jnp.maximum(previous, jnp.max(scores, axis=2))
        faded = jnp.exp(previous - peak_new)
        raised = jnp.exp(scores - peak_new[:, :, None])
        weight = weight * faded + jnp.sum(raised, axis=2)
        accumulated = accumulated * faded.T[:, :, None] + jnp.einsum(
            "hqk,khd->qhd",
            raised.astype(jnp.bfloat16),
            value_rows,
            preferred_element_type=jnp.float32,
        )
        updated += [peak_new, weight, accumulated]
    return tuple(updated)


def absorb_rows(running, portion, context_flags, queries, bias_heads):
    row_count = portion.shape[0]
    block_len = block_size(row_count)
    if block_len == row_count:
        return absorb(running, portion, context_flags, queries, bias_heads)
    stacked = portion.reshape(row_count // block_len, block_len, portion.shape[1])
    flag_blocks = context_flags.reshape(row_count // block_len, block_len)

    def advance(state_now, operand):
        return (absorb(state_now, operand[0], operand[1], queries, bias_heads), None)

    running, unused = lax.scan(advance, running, (stacked, flag_blocks))
    return running


def per_device(
    latent,
    context,
    conditioning,
    norm_gain,
    mod_shift,
    mod_scale,
    mod_gate,
    w_query,
    w_key,
    w_value,
    w_out,
    lambdas,
    context_bias,
    head_gain,
):
    head_dim = head_gain.shape[0] // 2
    head_count = lambdas.shape[0]
    rows_sp = mod_shift.shape[0]
    cond_rows = lax.dynamic_slice_in_dim(conditioning, lax.axis_index("sp") * rows_sp, rows_sp, 1)
    activated = jax.nn.silu(cond_rows).astype(jnp.bfloat16)
    partials = jnp.stack(
        [
            jnp.dot(activated, matrix, preferred_element_type=jnp.float32)
            for matrix in (mod_shift, mod_scale, mod_gate)
        ],
        axis=1,
    )
    summed = lax.psum(partials, "sp")
    modulation = lax.all_gather(summed, "tp", axis=2, tiled=True)
    own_rows = modulated(latent, norm_gain, modulation[0, 0], modulation[0, 1])
    context_rows = modulated(context, norm_gain, modulation[1, 0], modulation[1, 1])
    key_value = jnp.concatenate([w_key, w_value], axis=1)
    projector = jnp.concatenate([w_query, key_value], axis=1)
    projected = jnp.dot(
        lax.all_gather(own_rows, "tp", axis=0, tiled=True),
        projector,
        preferred_element_type=jnp.float32,
    ).astype(jnp.bfloat16)
    head_cols = w_query.shape[1]
    token_count = projected.shape[0]
    queries = projected[:, :head_cols].reshape(token_count, head_count, 2, head_dim)
    latent_kv = projected[:, head_cols:]
    context_kv = jnp.dot(context_rows, key_value, preferred_element_type=jnp.float32).astype(
        jnp.bfloat16
    )
    first_map = (
        jnp.full((head_count, token_count), NEGATIVE, jnp.float32),
        jnp.zeros((head_count, token_count), jnp.float32),
        jnp.zeros((token_count, head_count, 2 * head_dim), jnp.float32),
    )
    initial = first_map + first_map
    every_context = lax.all_gather(context_kv, "sp", axis=0, tiled=True)
    running = absorb_rows(
        initial,
        every_context,
        jnp.ones((every_context.shape[0],), jnp.float32),
        queries,
        context_bias,
    )
    portion = lax.all_gather(latent_kv, "sp", axis=0, tiled=True)
    running = absorb_rows(
        running, portion, jnp.zeros((portion.shape[0],), jnp.float32), queries, context_bias
    )
    peak_one, total_one, accum_one, peak_two, total_two, accum_two = running
    mixed = accum_one / total_one.T[:, :, None] - lambdas[None, :, None] * (
        accum_two / total_two.T[:, :, None]
    )
    normed = mixed * lax.rsqrt(jnp.mean(mixed * mixed, axis=-1, keepdims=True) + EPS) * head_gain
    flattened = normed.reshape(token_count, head_cols).astype(jnp.bfloat16)
    attended = lax.psum_scatter(
        jnp.dot(flattened, w_out, preferred_element_type=jnp.float32).astype(jnp.bfloat16),
        "tp",
        scatter_dimension=0,
        tiled=True,
    )
    return (latent.astype(jnp.float32) + modulation[0, 2] * attended.astype(jnp.float32)).astype(
        jnp.bfloat16
    )


def solution(mesh):
    return jax.shard_map(
        per_device,
        mesh=mesh,
        in_specs=(
            P(("sp", "tp"), None),
            P("sp", None),
            P(),
            P(),
            P("sp", "tp"),
            P("sp", "tp"),
            P("sp", "tp"),
            P(None, "tp"),
            P(None, "tp"),
            P(None, "tp"),
            P("tp", None),
            P("tp"),
            P("tp"),
            P(),
        ),
        out_specs=P(("sp", "tp"), None),
        check_vma=False,
    )
```

profile of v0, /device:TPU:0, one launch (start us, length us, event | category | flops | bytes accessed | tf_op | source)
XLA Modules:
  0.0 557.7 jit_solution(13907041467783386179)
XLA Ops:
  10.0 38.8 %psum.7 = f32[2,3,512]{2,0,1:T(2,128)S(1)} all-reduce(f32[2,3,512]{2,0,1:T(2,128)S(1)} %pad_maximum_fusion), channel_id=1, replica_groups=mesh['sp'=8,'tp'=4] {'sp'}, use_global_device_ids=true, to_apply=%region_0.1 | all-reduce | flops 3072 | bytes 24576 | tf_op jit(solution)/shard_map/psum | solution.py:101
  48.9 5.2 all_gather.12
  59.8 4.0 fusion.57
  63.9 20.6 %all-gather.4.cloned.1.call-done = bf16[768,2048]{1,0:T(8,128)(2,1)} async-done(((bf16[192,2048]{1,0:T(8,128)(2,1)}), bf16[768,2048]{1,0:T(8,128)(2,1)}) %all-gather.4.cloned.1.call-update) | async-done | bytes 3145744 | tf_op jit(solution)/shard_map/all_gather | solution.py:108
  84.5 8.8 %fusion.44 = bf16[768,1536]{1,0:T(8,128)(2,1)S(1)} fusion(bf16[768,2048]{1,0:T(8,128)(2,1)} %all-gather.4.cloned.1.call-done, bf16[2048,512]{1,0:T(8,128)(2,1)} %param.25, bf16[2048,512]{1,0:T(8,128)(2,1)} %param.24, bf16[2048,512]{1,0:T(8,128)(2,1)} %param.23), kind=kOutput, calls=%fused_computation.56 | convolution fusion | flops 4851892224 | bytes 11796480 | tf_op jit(solution)/shard_map/dot_general | solution.py:107
  96.4 39.3 %all-gather.6.cloned.1.call-done = bf16[1024,1024]{1,0:T(8,128)(2,1)} async-done(((bf16[128,1024]{1,0:T(8,128)(2,1)}), bf16[1024,1024]{1,0:T(8,128)(2,1)}) %all-gather.6.cloned.1.call-update) | async-done | bytes 2097168 | tf_op jit(solution)/shard_map/all_gather | solution.py:125
  149.7 6.2 %fusion.25 = (f32[4,768]{1,0:T(4,128)S(1)}, f32[4,768]{1,0:T(4,128)S(1)}, f32[4,768,1024]{2,1,0:T(8,128)}) fusion(f32[4]{0:T(128)S(1)} %copy-done.9, f32[4,768,1024]{2,1,0:T(8,128)S(1)} %fusion.67, bf16[1024,4,2,64]{0,3,2,1:T(8,128)(2,1)S(1)} %bitcast.155, bf16[768,4,2,64]{0,3,2,1:T(8,128)(2,1)S(1)} %bitcast.153), kind=kOutput, calls=%fused_computation.39 | convolution fusion | flops 421521408 | bytes 26108416 | tf_op jit(solution)/shard_map/qhd,khd->hqk/dot_general | solution.py:35
  155.8 8.2 %fusion.29 = (f32[4,768]{1,0:T(4,128)S(1)}, f32[4,768]{1,0:T(4,128)S(1)}) fusion(f32[4,768,1024]{2,1,0:T(8,128)} %get-tuple-element.134, f32[4,768]{1,0:T(4,128)S(1)} %broadcast_maximum_fusion, f32[4]{0:T(128)S(1)} %copy-done.9, f32[4,768]{1,0:T(4,128)S(1)} %broadcast_maximum_fusion.1, f32[4,768,1024]{2,1,0:T(8,128)S(1)} %fusion.67), kind=kLoop, calls=%fused_computation.43 | loop fusion | flops 25159680 | bytes 25214992 | tf_op jit(solution)/shard_map/reduce_sum | solution.py:47
  164.0 8.6 %bitcast_add_fusion.2 = f32[768,4,128]{0,2,1:T(8,128)} fusion(bf16[1024,4,128]{0,2,1:T(8,128)(2,1)S(1)} %bitcast.156, f32[4,768,1024]{2,1,0:T(8,128)} %get-tuple-element.134, f32[4,768]{1,0:T(4,128)S(1)} %broadcast_maximum_fusion, f32[4]{0:T(128)S(1)} %copy-done.9, f32[768,4]{0,1:T(4,128)S(1)} %get-tuple-element.136), kind=kOutput, calls=%fused_computation.67 | convolution fusion | flops 818282496 | bytes 15228944 | tf_op jit(solution)/shard_map/hqk,khd->qhd/dot_general | solution.py:48
  172.7 4.1 bitcast_add_fusion.3
  176.8 135.7 %all-gather.8.cloned.1.call-done = bf16[6144,1024]{1,0:T(8,128)(2,1)} async-done(((bf16[768,1024]{1,0:T(8,128)(2,1)}), bf16[6144,1024]{1,0:T(8,128)(2,1)}) %all-gather.8.cloned.1.call-update) | async-done | bytes 12582928 | tf_op jit(solution)/shard_map/all_gather | solution.py:133
  312.6 193.9 %while.20 = (s32[]{:T(128)}, f32[4,768]{1,0:T(4,128)S(1)}, f32[4,768]{1,0:T(4,128)S(1)}, f32[768,4,128]{0,2,1:T(8,128)}, f32[4,768]{1,0:T(4,128)S(1)}, /*index=5...) while((s32[]{:T(128)}, f32[4,768]{1,0:T(4,128)S(1)}, ...), condition=%wide.region_12.13_spmd, body=%wide.region_7.12_spmd.sunk | while | flops 2486716416 | bytes 128058136 | solution.py:69
  315.7 3.9 copy.54
  325.1 5.5 bitcast_reduce_fusion.3
  330.7 5.8 %bitcast_add_fusion.7 = f32[768,4,128]{0,2,1:T(8,128)} fusion(f32[768,4,128]{0,2,1:T(8,128)} %get-tuple-element.241, bf16[1024,4,128]{0,2,1:T(8,128)(2,1)} %bitcast.148, f32[4,1024,768]{2,1,0:T(8,128)S(1)} %get-tuple-element.214, f32[4,768]{1,0:T(4,128)S(1)} %get-tuple-element.250, f32[4]{0:T(128)S(1)} %broadcast_multiply_fusion.2, ...), kind=kOutput, calls=%fused_computation.14.clone.1 | convolution fusion | flops 818675712 | bytes 16801808 | tf_op jit(solution)/shard_map/while/body/eval_jaxpr/hqk,khd->qhd/dot_general | solution.py:48
  339.7 5.1 fusion.118
  357.5 5.5 bitcast_reduce_fusion.3
  363.0 5.8 %bitcast_add_fusion.7 = f32[768,4,128]{0,2,1:T(8,128)} fusion(f32[768,4,128]{0,2,1:T(8,128)} %get-tuple-element.241, bf16[1024,4,128]{0,2,1:T(8,128)(2,1)} %bitcast.148, f32[4,1024,768]{2,1,0:T(8,128)S(1)} %get-tuple-element.214, f32[4,768]{1,0:T(4,128)S(1)} %get-tuple-element.250, f32[4]{0:T(128)S(1)} %broadcast_multiply_fusion.2, ...), kind=kOutput, calls=%fused_computation.14.clone.1 | convolution fusion | flops 818675712 | bytes 16801808 | tf_op jit(solution)/shard_map/while/body/eval_jaxpr/hqk,khd->qhd/dot_general | solution.py:48
  372.0 5.1 fusion.118
  389.8 5.5 bitcast_reduce_fusion.3
  395.3 5.8 %bitcast_add_fusion.7 = f32[768,4,128]{0,2,1:T(8,128)} fusion(f32[768,4,128]{0,2,1:T(8,128)} %get-tuple-element.241, bf16[1024,4,128]{0,2,1:T(8,128)(2,1)} %bitcast.148, f32[4,1024,768]{2,1,0:T(8,128)S(1)} %get-tuple-element.214, f32[4,768]{1,0:T(4,128)S(1)} %get-tuple-element.250, f32[4]{0:T(128)S(1)} %broadcast_multiply_fusion.2, ...), kind=kOutput, calls=%fused_computation.14.clone.1 | convolution fusion | flops 818675712 | bytes 16801808 | tf_op jit(solution)/shard_map/while/body/eval_jaxpr/hqk,khd->qhd/dot_general | solution.py:48
  404.3 5.1 fusion.118
  422.1 5.5 bitcast_reduce_fusion.3
  427.6 5.8 %bitcast_add_fusion.7 = f32[768,4,128]{0,2,1:T(8,128)} fusion(f32[768,4,128]{0,2,1:T(8,128)} %get-tuple-element.241, bf16[1024,4,128]{0,2,1:T(8,128)(2,1)} %bitcast.148, f32[4,1024,768]{2,1,0:T(8,128)S(1)} %get-tuple-element.214, f32[4,768]{1,0:T(4,128)S(1)} %get-tuple-element.250, f32[4]{0:T(128)S(1)} %broadcast_multiply_fusion.2, ...), kind=kOutput, calls=%fused_computation.14.clone.1 | convolution fusion | flops 818675712 | bytes 16801808 | tf_op jit(solution)/shard_map/while/body/eval_jaxpr/hqk,khd->qhd/dot_general | solution.py:48
  436.6 5.1 fusion.118
  454.4 5.5 bitcast_reduce_fusion.3
  459.9 5.8 %bitcast_add_fusion.7 = f32[768,4,128]{0,2,1:T(8,128)} fusion(f32[768,4,128]{0,2,1:T(8,128)} %get-tuple-element.241, bf16[1024,4,128]{0,2,1:T(8,128)(2,1)} %bitcast.148, f32[4,1024,768]{2,1,0:T(8,128)S(1)} %get-tuple-element.214, f32[4,768]{1,0:T(4,128)S(1)} %get-tuple-element.250, f32[4]{0:T(128)S(1)} %broadcast_multiply_fusion.2, ...), kind=kOutput, calls=%fused_computation.14.clone.1 | convolution fusion | flops 818675712 | bytes 16801808 | tf_op jit(solution)/shard_map/while/body/eval_jaxpr/hqk,khd->qhd/dot_general | solution.py:48
  469.0 5.1 fusion.118
  486.7 5.5 bitcast_reduce_fusion.3
  492.3 5.8 %bitcast_add_fusion.7 = f32[768,4,128]{0,2,1:T(8,128)} fusion(f32[768,4,128]{0,2,1:T(8,128)} %get-tuple-element.241, bf16[1024,4,128]{0,2,1:T(8,128)(2,1)} %bitcast.148, f32[4,1024,768]{2,1,0:T(8,128)S(1)} %get-tuple-element.214, f32[4,768]{1,0:T(4,128)S(1)} %get-tuple-element.250, f32[4]{0:T(128)S(1)} %broadcast_multiply_fusion.2, ...), kind=kOutput, calls=%fused_computation.14.clone.1 | convolution fusion | flops 818675712 | bytes 16801808 | tf_op jit(solution)/shard_map/while/body/eval_jaxpr/hqk,khd->qhd/dot_general | solution.py:48
  501.3 5.1 fusion.118
  512.7 36.2 %reduce-scatter.2.cloned.1.call-done = bf16[192,2048]{1,0:T(8,128)(2,1)} async-done(((bf16[768,2048]{1,0:T(8,128)(2,1)}), bf16[192,2048]{1,0:T(8,128)(2,1)}) %reduce-scatter.2.cloned.1.call-update) | async-done | bytes 786448 | tf_op jit(solution)/shard_map/reduce_scatter | solution.py:143
  (153 shorter events, 125.8 us)
Async XLA Ops:
  6.5 502.6 %copy-start = (bf16[512,2048]{1,0:T(8,128)(2,1)S(1)}, bf16[512,2048]{1,0:T(8,128)(2,1)}, u32[]{:S(2)}) copy-start(bf16[512,2048]{1,0:T(8,128)(2,1)} %param.26) | copy-start | bytes 6291460
  6.5 77.9 %all-gather.4.cloned.1.call-start = ((), (), s32[]{:S(2)}) async-start(), calls=%async_computation.1 | async-start | bytes 3932160 | tf_op jit(solution)/shard_map/all_gather | solution.py:108
  58.5 77.2 %all-gather.6.cloned.1.call-start = ((), (), s32[]{:S(2)}) async-start(), calls=%async_computation.2 | async-start | bytes 2359296 | tf_op jit(solution)/shard_map/all_gather | solution.py:125
  63.8 248.7 %all-gather.8.cloned.1.call-start = ((), (), s32[]{:S(2)}) async-start(), calls=%async_computation.3 | async-start | bytes 14155776 | tf_op jit(solution)/shard_map/all_gather | solution.py:133
  93.2 1.4 copy-start.4
  96.2 452.7 %reduce-scatter.2.cloned.1.call-start = ((), (), s32[]{:S(2)}) async-start(), calls=%async_computation.4 | async-start | bytes 3932160 | tf_op jit(solution)/shard_map/reduce_scatter | solution.py:143
  146.5 3.1 copy-start.3
  146.5 3.1 copy-start.9
  155.8 8.2 %copy-start.7 = (bf16[1024,512]{0,1:T(8,128)(2,1)S(1)}, bf16[1024,512]{0,1:T(8,128)(2,1)}, u32[]{:S(2)}) copy-start(bf16[1024,512]{0,1:T(8,128)(2,1)} %copy.41) | copy-start | bytes 3145732
  312.6 193.9 %copy-start.10 = (f32[4]{0:T(128)S(1)}, f32[4]{0:T(128)}, u32[]{:S(2)}) copy-start(f32[4]{0:T(128)} %param.27) | copy-start | bytes 52
  312.6 196.2 %copy-start.11 = (f32[128]{0:T(128)S(1)}, f32[128]{0:T(128)}, u32[]{:S(2)}) copy-start(f32[128]{0:T(128)} %param.29) | copy-start | bytes 1540
  330.6 5.8 %copy-start.1 = (bf16[1024,512]{0,1:T(8,128)(2,1)S(1)}, bf16[1024,512]{0,1:T(8,128)(2,1)}, u32[]{:S(2)}) copy-start(bf16[1024,512]{0,1:T(8,128)(2,1)} %get-tuple-element.220) | copy-start | bytes 3145732 | tf_op jit(solution)/shard_map/while
  330.6 5.8 %copy-start.5 = (f32[768,4,128]{0,2,1:T(8,128)S(1)}, f32[768,4,128]{0,2,1:T(8,128)}, u32[]{:S(2)}) copy-start(f32[768,4,128]{0,2,1:T(8,128)} %get-tuple-element.238) | copy-start | bytes 4718596 | tf_op jit(solution)/shard_map/while
  339.7 5.2 copy-start.6
  363.0 5.8 %copy-start.1 = (bf16[1024,512]{0,1:T(8,128)(2,1)S(1)}, bf16[1024,512]{0,1:T(8,128)(2,1)}, u32[]{:S(2)}) copy-start(bf16[1024,512]{0,1:T(8,128)(2,1)} %get-tuple-element.220) | copy-start | bytes 3145732 | tf_op jit(solution)/shard_map/while
  363.0 5.8 %copy-start.5 = (f32[768,4,128]{0,2,1:T(8,128)S(1)}, f32[768,4,128]{0,2,1:T(8,128)}, u32[]{:S(2)}) copy-start(f32[768,4,128]{0,2,1:T(8,128)} %get-tuple-element.238) | copy-start | bytes 4718596 | tf_op jit(solution)/shard_map/while
  372.0 5.2 copy-start.6
  395.3 5.8 %copy-start.1 = (bf16[1024,512]{0,1:T(8,128)(2,1)S(1)}, bf16[1024,512]{0,1:T(8,128)(2,1)}, u32[]{:S(2)}) copy-start(bf16[1024,512]{0,1:T(8,128)(2,1)} %get-tuple-element.220) | copy-start | bytes 3145732 | tf_op jit(solution)/shard_map/while
  395.3 5.8 %copy-start.5 = (f32[768,4,128]{0,2,1:T(8,128)S(1)}, f32[768,4,128]{0,2,1:T(8,128)}, u32[]{:S(2)}) copy-start(f32[768,4,128]{0,2,1:T(8,128)} %get-tuple-element.238) | copy-start | bytes 4718596 | tf_op jit(solution)/shard_map/while
  404.3 5.2 copy-start.6
  427.6 5.8 %copy-start.1 = (bf16[1024,512]{0,1:T(8,128)(2,1)S(1)}, bf16[1024,512]{0,1:T(8,128)(2,1)}, u32[]{:S(2)}) copy-start(bf16[1024,512]{0,1:T(8,128)(2,1)} %get-tuple-element.220) | copy-start | bytes 3145732 | tf_op jit(solution)/shard_map/while
  427.6 5.8 %copy-start.5 = (f32[768,4,128]{0,2,1:T(8,128)S(1)}, f32[768,4,128]{0,2,1:T(8,128)}, u32[]{:S(2)}) copy-start(f32[768,4,128]{0,2,1:T(8,128)} %get-tuple-element.238) | copy-start | bytes 4718596 | tf_op jit(solution)/shard_map/while
  436.6 5.2 copy-start.6
  459.9 5.8 %copy-start.1 = (bf16[1024,512]{0,1:T(8,128)(2,1)S(1)}, bf16[1024,512]{0,1:T(8,128)(2,1)}, u32[]{:S(2)}) copy-start(bf16[1024,512]{0,1:T(8,128)(2,1)} %get-tuple-element.220) | copy-start | bytes 3145732 | tf_op jit(solution)/shard_map/while
  459.9 5.8 %copy-start.5 = (f32[768,4,128]{0,2,1:T(8,128)S(1)}, f32[768,4,128]{0,2,1:T(8,128)}, u32[]{:S(2)}) copy-start(f32[768,4,128]{0,2,1:T(8,128)} %get-tuple-element.238) | copy-start | bytes 4718596 | tf_op jit(solution)/shard_map/while
  468.9 5.2 copy-start.6
  492.2 5.8 %copy-start.1 = (bf16[1024,512]{0,1:T(8,128)(2,1)S(1)}, bf16[1024,512]{0,1:T(8,128)(2,1)}, u32[]{:S(2)}) copy-start(bf16[1024,512]{0,1:T(8,128)(2,1)} %get-tuple-element.220) | copy-start | bytes 3145732 | tf_op jit(solution)/shard_map/while
  492.2 5.8 %copy-start.5 = (f32[768,4,128]{0,2,1:T(8,128)S(1)}, f32[768,4,128]{0,2,1:T(8,128)}, u32[]{:S(2)}) copy-start(f32[768,4,128]{0,2,1:T(8,128)} %get-tuple-element.238) | copy-start | bytes 4718596 | tf_op jit(solution)/shard_map/while
  501.3 5.2 copy-start.6
  509.1 39.8 %copy-start.2 = (bf16[192,2048]{1,0:T(8,128)(2,1)S(1)}, bf16[192,2048]{1,0:T(8,128)(2,1)}, u32[]{:S(2)}) copy-start(bf16[192,2048]{1,0:T(8,128)(2,1)} %param.16) | copy-start | bytes 2359300
  509.1 39.8 %copy-start.8 = (f32[1,1,2048]{2,0,1:T(1,128)S(1)}, f32[1,1,2048]{2,0,1:T(1,128)}, u32[]{:S(2)}) copy-start(f32[1,1,2048]{2,0,1:T(1,128)} %get-tuple-element.125) | copy-start | bytes 24580
Sparse Core Ops, SparseCore 0:
  58.6 25.7 all-gather.3
  86.6 49.0 all-gather.5
  137.9 174.6 all-gather.7
  512.8 36.0 reduce-scatter.1
where the time goes:
time: 559 us; the launch traced here: 558 us
  waiting for transfers between devices  232 us (42%)
  matrix products  145 us (26%)
  local copies, waits for them, and re-layouts  72.2 us (13%)
  other arithmetic  49.9 us (9%)
  blocking collectives  44 us (8%)
  between operations  13.3 us (2%)
    all_gather x1, waiting for transfers between devices, per_device(): portion = lax.all_gather(latent_kv, 'sp', axis=0, tiled=True)  136 us
    dot_general x14, matrix products, absorb(): jnp.einsum('hqk,khd->qhd', raised.astype(jnp.bfloat16), value_rows, prefe...  66.5 us
    dot_general x14, matrix products, absorb(): jnp.einsum('qhd,khd->hqk', queries[:, :, which_map], key_rows[:, :, which...  59 us
    dynamic_slice x12, local copies, waits for them, and re-layouts, absorb_rows(): running, unused = lax.scan(advance, running, (stacked, flag_blocks))  42.2 us
    all_gather x1, waiting for transfers between devices, per_device(): every_context = lax.all_gather(context_kv, 'sp', axis=0, tiled=True)  39.3 us
    reduce_sum x7, other arithmetic, absorb(): weight = weight * faded + jnp.sum(raised, axis=2)  39 us
    psum x1, blocking collectives, per_device(): summed = lax.psum(partials, 'sp')  38.8 us
    reduce_scatter x1, waiting for transfers between devices, per_device(): lax.psum_scatter(jnp.dot(flattened, w_out, preferred_element_type=jnp.flo...  36.2 us
  transfers between devices with their start and end apart: 4, of which 4 were waited for; matrix products, arithmetic and copies ran while one was open for 10% of the time, Pallas kernels for 0%

commit v1 on v0

v1 whole, which is shorter than its diff:
```python
import functools
import math

import jax
import jax.numpy as jnp
from jax import lax
from jax.experimental import pallas as pl
from jax.experimental.pallas import tpu as pltpu
from jax.sharding import Mesh
from jax.sharding import PartitionSpec as P

EPS = 1e-06
LOG2E = 1.4426950408889634
NT = (((1,), (1,)), ((), ()))
VMEM_LIMIT = 60 * 1024 * 1024


def params(*semantics):
    return pltpu.CompilerParams(dimension_semantics=semantics, vmem_limit_bytes=VMEM_LIMIT)


def whole_spec(shape):
    return pl.BlockSpec(shape, lambda i: (0,) * len(shape))


def project_kernel(ctx, heads, width, lat_ref, ctx_ref, mod_ref, wq_ref, wk_ref, wv_ref, q_ref, kv_ref, hid_ref):
    @pl.when(pl.program_id(0) == 0)
    def _():
        def norm(src_ref, which, start, rows):
            x = src_ref[pl.ds(start, rows), :].astype(jnp.float32)
            inv = lax.rsqrt(jnp.mean(x * x, axis=-1, keepdims=True) + EPS)
            out = x * inv * mod_ref[which, 0:1, :] + mod_ref[which, 1:2, :]
            return out.astype(jnp.bfloat16)

        step = math.gcd(ctx, 64)

        def ctx_body(i, carry):
            hid_ref[pl.ds(pl.multiple_of(i * step, step), step), :] = norm(
                ctx_ref, 1, pl.multiple_of(i * step, step), step
            )
            return carry

        lax.fori_loop(0, ctx // step, ctx_body, 0)
        lat = lat_ref.shape[0]
        lstep = math.gcd(lat, 64)

        def lat_body(i, carry):
            at = pl.multiple_of(i * lstep, lstep)
            hid_ref[pl.ds(ctx + at, lstep), :] = norm(lat_ref, 0, at, lstep)
            return carry

        lax.fori_loop(0, lat // lstep, lat_body, 0)

    hidden = hid_ref[...]
    q = jnp.dot(hidden[ctx:], wq_ref[...], preferred_element_type=jnp.float32).astype(jnp.bfloat16)
    k = jnp.dot(hidden, wk_ref[...], preferred_element_type=jnp.float32).astype(jnp.bfloat16)
    v = jnp.dot(hidden, wv_ref[...], preferred_element_type=jnp.float32).astype(jnp.bfloat16)
    for h in range(heads):
        cols = slice(h * width, (h + 1) * width)
        q_ref[h] = q[:, cols]
        kv_ref[h, :, :width] = k[:, cols]
        kv_ref[h, :, width:] = v[:, cols]


def project(latent, context, mods, w_query, w_key, w_value, head_count, width):
    lat, dim = latent.shape
    ctx = context.shape[0]
    per = 2 if head_count % 2 == 0 else 1
    weight = pl.BlockSpec((dim, per * width), lambda i: (0, i))
    return pl.pallas_call(
        functools.partial(project_kernel, ctx, per, width),
        grid=(head_count // per,),
        in_specs=[
            whole_spec((lat, dim)),
            whole_spec((ctx, dim)),
            whole_spec(mods.shape),
            weight,
            weight,
            weight,
        ],
        out_specs=[
            pl.BlockSpec((per, lat, width), lambda i: (i, 0, 0)),
            pl.BlockSpec((per, ctx + lat, 2 * width), lambda i: (i, 0, 0)),
        ],
        out_shape=[
            jax.ShapeDtypeStruct((head_count, lat, width), jnp.bfloat16),
            jax.ShapeDtypeStruct((head_count, ctx + lat, 2 * width), jnp.bfloat16),
        ],
        scratch_shapes=[pltpu.VMEM((ctx + lat, dim), jnp.bfloat16)],
        compiler_params=params("arbitrary"),
        cost_estimate=pl.CostEstimate(
            flops=6 * (ctx + lat) * dim * head_count * width,
            bytes_accessed=2 * dim * (lat + ctx + 3 * head_count * width),
            transcendentals=0,
        ),
        name="project",
    )(latent, context, mods, w_query, w_key, w_value)


def attend_kernel(ctx, first, last, *refs):
    refs = list(refs)
    scal_ref, q_ref, kv_ref = refs[:3]
    at = 3
    if not first:
        ml_in, acc_in = refs[at : at + 2]
        at += 2
    if last:
        gain_ref, out_ref = refs[at : at + 2]
    else:
        ml_out, acc_out = refs[at : at + 2]
    rows, width = q_ref.shape
    sources, keys = kv_ref.shape[0], kv_ref.shape[1]
    half = width // 2
    scaled = q_ref[...].astype(jnp.float32) * (half ** (-0.5) * LOG2E)
    high = scaled.astype(jnp.bfloat16)
    low = (scaled - high.astype(jnp.float32)).astype(jnp.bfloat16)
    lanes = lax.broadcasted_iota(jnp.int32, (rows, width), 1)
    zero = jnp.zeros_like(high)
    bias = scal_ref[1]
    if ctx % 128:
        flags = lax.broadcasted_iota(jnp.int32, (1, keys), 1) < ctx
        bias_row = jnp.where(flags, bias, 0.0)
    sides = []
    for which in range(2):
        keep = (lanes < half) if which == 0 else (lanes >= half)
        sides.append(
            jnp.concatenate([jnp.where(keep, high, zero), jnp.where(keep, low, zero)], axis=1)
        )
    state = []
    for which in range(2):
        if first:
            state.append(None)
        else:
            ml = ml_in[which]
            state.append((ml[:, 0:1], ml[:, half : half + 1], acc_in[which]))
    for source in range(sources):
        k = kv_ref[source, :, :width]
        v = kv_ref[source, :, width:]
        doubled = jnp.concatenate([k, k], axis=1)
        for which in range(2):
            s = lax.dot_general(sides[which], doubled, NT, preferred_element_type=jnp.float32)
            if ctx % 128:
                s = s + bias_row
            else:
                s = jnp.concatenate([s[:, :ctx] + bias, s[:, ctx:]], axis=1)
            top = jnp.max(s, axis=1, keepdims=True)
            if state[which] is None:
                p = jnp.exp2(s - top)
                total = jnp.sum(p, axis=1, keepdims=True)
                acc = jnp.dot(p.astype(jnp.bfloat16), v, preferred_element_type=jnp.float32)
            else:
                old, total, acc = state[which]
                top = jnp.maximum(old, top)
                fade = jnp.exp2(old - top)
                p = jnp.exp2(s - top)
                total = total * fade + jnp.sum(p, axis=1, keepdims=True)
                acc = acc * fade + jnp.dot(
                    p.astype(jnp.bfloat16), v, preferred_element_type=jnp.float32
                )
            state[which] = (top, total, acc)
    if last:
        mixed = state[0][2] / state[0][1] - scal_ref[0] * (state[1][2] / state[1][1])
        normed = mixed * lax.rsqrt(jnp.mean(mixed * mixed, axis=-1, keepdims=True) + EPS)
        out_ref[...] = (normed * gain_ref[...]).astype(jnp.bfloat16)
    else:
        for which in range(2):
            top, total, acc = state[which]
            ml_out[which] = jnp.where(lanes < half, top, total)
            acc_out[which] = acc


def attend(ctx, scalars, queries, kv, carried, gain, last):
    tokens, width = queries.shape
    block = math.gcd(tokens, 256)
    first = carried is None
    row_spec = pl.BlockSpec((block, width), lambda i: (i, 0))
    state_spec = pl.BlockSpec((2, block, width), lambda i: (0, i, 0))
    in_specs = [pl.BlockSpec(memory_space=pltpu.SMEM), row_spec, whole_spec(kv.shape)]
    operands = [scalars, queries, kv]
    if not first:
        in_specs += [state_spec, state_spec]
        operands += list(carried)
    if last:
        in_specs.append(whole_spec((1, width)))
        operands.append(gain)
        out_specs = row_spec
        out_shape = jax.ShapeDtypeStruct((tokens, width), jnp.bfloat16)
    else:
        out_specs = [state_spec, state_spec]
        out_shape = [jax.ShapeDtypeStruct((2, tokens, width), jnp.float32)] * 2
    key_count = kv.shape[0] * kv.shape[1]
    return pl.pallas_call(
        functools.partial(attend_kernel, ctx, first, last),
        grid=(tokens // block,),
        in_specs=in_specs,
        out_specs=out_specs,
        out_shape=out_shape,
        compiler_params=params("arbitrary"),
        cost_estimate=pl.CostEstimate(
            flops=16 * tokens * key_count * width,
            bytes_accessed=2 * key_count * 2 * width + 8 * tokens * width,
            transcendentals=2 * tokens * key_count,
        ),
        name="attend",
    )(*operands)


def finish_kernel(head_count, groups, recv_ref, w_ref, lat_ref, gate_ref, out_ref):
    rows_w = w_ref.shape[0] // groups
    summed = None
    for t in range(groups):
        left = jnp.concatenate([recv_ref[a * groups + t] for a in range(head_count)], axis=1)
        part = jnp.dot(
            left, w_ref[t * rows_w : (t + 1) * rows_w, :], preferred_element_type=jnp.float32
        ).astype(jnp.bfloat16)
        part = part.astype(jnp.float32)
        summed = part if summed is None else summed + part
    attended = summed.astype(jnp.bfloat16).astype(jnp.float32)
    out_ref[...] = (lat_ref[...].astype(jnp.float32) + gate_ref[...] * attended).astype(jnp.bfloat16)


def finish(recv, w_full, latent, gate, head_count, groups):
    rows, dim = latent.shape
    block = math.gcd(dim, 512)
    return pl.pallas_call(
        functools.partial(finish_kernel, head_count, groups),
        grid=(dim // block,),
        in_specs=[
            whole_spec(recv.shape),
            pl.BlockSpec((w_full.shape[0], block), lambda i: (0, i)),
            pl.BlockSpec((rows, block), lambda i: (0, i)),
            pl.BlockSpec((1, block), lambda i: (0, i)),
        ],
        out_specs=pl.BlockSpec((rows, block), lambda i: (0, i)),
        out_shape=jax.ShapeDtypeStruct((rows, dim), jnp.bfloat16),
        compiler_params=params("arbitrary"),
        cost_estimate=pl.CostEstimate(
            flops=2 * rows * dim * w_full.shape[0],
            bytes_accessed=2 * dim * w_full.shape[0],
            transcendentals=0,
        ),
        name="finish",
    )(recv, w_full, latent, gate)


def per_device(
    latent,
    context,
    conditioning,
    norm_gain,
    mod_shift,
    mod_scale,
    mod_gate,
    w_query,
    w_key,
    w_value,
    w_out,
    lambdas,
    context_bias,
    head_gain,
):
    width = head_gain.shape[0]
    head_count = lambdas.shape[0]
    parts = lax.axis_size("part")
    tp = lax.axis_size("tp")
    ctx = context.shape[0]
    rows_sp = mod_shift.shape[0]
    sp_at = lax.axis_index(("head", "part"))
    cond_rows = lax.dynamic_slice_in_dim(conditioning, sp_at * rows_sp, rows_sp, 1)
    activated = jax.nn.silu(cond_rows).astype(jnp.bfloat16)
    partials = jnp.concatenate(
        [
            jnp.dot(activated, matrix, preferred_element_type=jnp.float32)
            for matrix in (mod_shift, mod_scale, mod_gate)
        ],
        axis=0,
    )
    gathered = lax.all_gather(partials, ("head", "part", "tp"), axis=0)
    summed = jnp.sum(gathered.reshape(-1, tp, 3, 2, partials.shape[1]), axis=0)
    modulation = jnp.moveaxis(summed, 0, 2).reshape(3, 2, -1)
    factors = norm_gain * (1.0 + modulation[1])
    mods = jnp.stack([factors, modulation[0]], axis=1)
    rows = lax.all_gather(latent, "tp", axis=0, tiled=True)
    w_full = lax.all_gather(w_out, "tp", axis=0, tiled=True)
    queries, kv = project(rows, context, mods, w_query, w_key, w_value, head_count, width)
    kv = lax.all_to_all(kv, "head", 0, 0, tiled=True)
    remote = [
        lax.ppermute(kv, "part", [(i, (i - j) % parts) for i in range(parts)])
        for j in range(1, parts)
    ]
    queries = lax.all_to_all(queries, "head", 0, 0, tiled=True)
    queries = queries.reshape(-1, width)
    head_at = lax.axis_index("head")
    scalars = jnp.stack([lambdas[head_at], context_bias[head_at] * LOG2E])
    gain = head_gain.reshape(1, width)
    carried = None
    blocks = [kv] + remote
    for j, block in enumerate(blocks):
        carried = attend(ctx, scalars, queries, block, carried, gain, j == len(blocks) - 1)
    normed = carried.reshape(head_count * tp, latent.shape[0], width)
    recv = lax.all_to_all(normed, ("head", "tp"), 0, 0, tiled=True)
    return finish(recv, w_full, latent, modulation[2, 0:1], head_count, tp)


def solution(mesh):
    sp, tp = mesh.shape["sp"], mesh.shape["tp"]

    def run(*args):
        head_count = args[11].shape[0] // tp
        inner = Mesh(mesh.devices.reshape(head_count, sp // head_count, tp), ("head", "part", "tp"))
        seq = ("head", "part")
        every = ("head", "part", "tp")
        return jax.shard_map(
            per_device,
            mesh=inner,
            in_specs=(
                P(every, None),
                P(seq, None),
                P(),
                P(),
                P(seq, "tp"),
                P(seq, "tp"),
                P(seq, "tp"),
                P(None, "tp"),
                P(None, "tp"),
                P(None, "tp"),
                P("tp", None),
                P("tp"),
                P("tp"),
                P(),
            ),
            out_specs=P(every, None),
            check_vma=False,
        )(*args)

    return run
```

time: 559 us -> 289 us (0.52)
  waiting for transfers between devices: 232 us -> 35.9 us
  matrix products: 145 us -> 2.48 us
  Pallas kernels: 0 us -> 130 us
  local copies, waits for them, and re-layouts: 72.2 us -> 4.08 us
  blocking collectives: 44 us -> 92.1 us
  other arithmetic: 49.9 us -> 2.07 us
  starting transfers between devices: 0.31 us -> 7.33 us
    all_gather x3 -> x2, waiting for transfers between devices: 196 us -> 0.01 us  [the longest x1 0.01 us: per_device(): rows = lax.all_gather(latent, 'tp', axis=0, tiled=True)]
    dot_general x31 -> x0, matrix products: 142 us -> none  [the longest x14 66.5 us: absorb(): jnp.einsum('hqk,khd->qhd', raised.astype(jnp.bfloat16), value_rows, prefe...]
    pallas_call x0 -> x4, Pallas kernels: none -> 130 us  [the longest x2 111 us: attend(): pl.pallas_call(functools.partial(attend_kernel, ctx, first, last), grid=(...]
    all_to_all x0 -> x1, blocking collectives: none -> 47.1 us  [per_device(): kv = lax.all_to_all(kv, 'head', 0, 0, tiled=True)]
    reduce_sum x10 -> x1, other arithmetic: 43.9 us -> 0.13 us  [per_device(): summed = jnp.sum(gathered.reshape(-1, tp, 3, 2, partials.shape[1]), axis=0)]
    dynamic_slice x12 -> x2, local copies, waits for them, and re-layouts: 42.2 us -> 1.26 us  [per_device(): scalars = jnp.stack([lambdas[head_at], context_bias[head_at] * LOG2E])]
    all_gather x1, blocking collectives: 5.2 us -> 45.1 us  [per_device(): gathered = lax.all_gather(partials, ('head', 'part', 'tp'), axis=0)]
    psum x1 -> x0, blocking collectives: 38.8 us -> none  [per_device(): summed = lax.psum(partials, 'sp')]
  transfers between devices with their start and end apart: 4 -> 5, of which waited for: 4 -> 2; matrix products, arithmetic and copies ran while one was open for 10% -> 2% of each run, Pallas kernels for 0% -> 43%
where the time goes in v1:
time: 289 us; the launch traced here: 288 us
  Pallas kernels  130 us (45%)
  blocking collectives  92.1 us (32%)
  waiting for transfers between devices  35.9 us (12%)
  between operations  14.2 us (5%)
  starting transfers between devices  7.33 us (3%)
  local copies, waits for them, and re-layouts  4.08 us (1%)
    pallas_call x2, Pallas kernels, attend(): pl.pallas_call(functools.partial(attend_kernel, ctx, first, last), grid=(...  111 us
    all_to_all x1, blocking collectives, per_device(): kv = lax.all_to_all(kv, 'head', 0, 0, tiled=True)  47.1 us
    all_gather x1, blocking collectives, per_device(): gathered = lax.all_gather(partials, ('head', 'part', 'tp'), axis=0)  45.1 us
    all_to_all x1, waiting for transfers between devices, per_device(): recv = lax.all_to_all(normed, ('head', 'tp'), 0, 0, tiled=True)  18 us
    all_to_all x1, waiting for transfers between devices, per_device(): queries = lax.all_to_all(queries, 'head', 0, 0, tiled=True)  16.5 us
    pallas_call x1, Pallas kernels, project(): pl.pallas_call(functools.partial(project_kernel, ctx, per, width), grid=(...  13 us
    pallas_call x1, Pallas kernels, finish(): pl.pallas_call(functools.partial(finish_kernel, head_count, groups), grid...  6.56 us
  transfers between devices with their start and end apart: 5, of which 2 were waited for; matrix products, arithmetic and copies ran while one was open for 2% of the time, Pallas kernels for 43%

profile of v1, /device:TPU:0, one launch (start us, length us, event | category | flops | bytes accessed | tf_op | source)
XLA Modules:
  0.0 288.3 jit_solution(2224323669498599394)
XLA Ops:
  6.5 0.0 copy-start
  6.5 0.0 all-gather.5.cloned.1.call-start
  6.5 0.7 all-gather.5.cloned.1.call-update
  7.3 0.0 copy-start.6
  7.3 0.0 all-gather.7.cloned.1.call-start
  7.3 0.7 all-gather.7.cloned.1.call-update
  8.0 0.8 fusion.1
  8.9 0.8 fusion.3
  9.7 0.8 fusion.5
  10.6 45.1 %all-gather.1 = f32[32,6,512]{2,1,0:T(8,128)S(1)} all-gather(f32[1,6,512]{2,1,0:T(8,128)S(1)} %maximum_bitcast_fusion), channel_id=2, replica_groups=mesh['head'=4,'part'=2,'tp'=4] {'head','part','tp'}, dimensions={0}, use_global_device_ids=true | all-gather | bytes 405504 | tf_op jit(solution)/shard_map/all_gather | solution.py:278
  55.6 0.2 reshape.65
  55.9 0.1 reduce_sum.9
  56.1 0.6 pad_maximum_fusion.mod_ref
  56.8 13.0 %project.1 = (bf16[4,768,128]{2,1,0:T(8,128)(2,1)}, bf16[4,896,256]{2,1,0:T(8,128)(2,1)}) custom-call(bf16[768,2048]{1,0:T(8,128)(2,1)} %all-gather.5.cloned.1.call-done.lat_ref, bf16[128,2048]{1,0:T(8,128)(2,1)} %ctx_ref.1, f32[2,2,2048]{2,1,0:T(2,128)} %pad_maximum_fusion.mod_ref, bf16[2048,512]{1,0:T(8,128)(2,1)} %wq_ref.1, bf16[2048,512]{1,0:T(8,128)(2,1)} %wk_ref.1, ...), custom_call_target="tpu_custom_call" | custom-call | flops 5637144576 | bytes 9961472 | tf_op jit(solution)/shard_map/project/pallas_call | solution.py:70
  69.7 47.1 %all_to_all.15.refs_2_ = bf16[4,896,256]{2,1,0:T(8,128)(2,1)S(1)} all-to-all(bf16[4,896,256]{2,1,0:T(8,128)(2,1)} %get-tuple-element.10), channel_id=1, replica_groups=mesh['head'=4,'part'=2,'tp'=4] {'head'}, dimensions={0} | all-to-all | bytes 3670016 | tf_op jit(solution)/shard_map/all_to_all | solution.py:286
  116.8 3.7 %all-to-all-start = ((bf16[4,768,128]{2,1,0:T(8,128)(2,1)}), bf16[4,768,128]{2,1,0:T(8,128)(2,1)S(1)}, u32[]{:S(2)}, u32[]{:S(2)}) async-start(bf16[4,768,128]{2,1,0:T(8,128)(2,1)} %get-tuple-element.9), calls=%async_computation | async-start | bytes 1572864 | tf_op jit(solution)/shard_map/all_to_all | solution.py:291
  120.5 0.7 dynamic_slice.10
  121.2 0.6 dynamic_slice.9
  122.4 1.3 pad_maximum_fusion.1.refs_0_
  123.7 0.0 collective-permute-start
  123.7 16.5 %all-to-all-done = bf16[4,768,128]{2,1,0:T(8,128)(2,1)S(1)} async-done(((bf16[4,768,128]{2,1,0:T(8,128)(2,1)}), bf16[4,768,128]{2,1,0:T(8,128)(2,1)S(1)}, u32[]{:S(2)}, u32[]{:S(2)}) %all-to-all-start) | async-done | bytes 786464 | tf_op jit(solution)/shard_map/all_to_all | solution.py:291
  140.2 0.0 copy-done.2
  140.2 0.9 copy-done.3
  141.0 49.0 %attend.2 = (f32[2,3072,128]{2,1,0:T(8,128)}, f32[2,3072,128]{2,1,0:T(8,128)}) custom-call(f32[2]{0:T(128)} %pad_maximum_fusion.1.refs_0_, bf16[3072,128]{1,0:T(8,128)(2,1)} %bitcast.13, bf16[4,896,256]{2,1,0:T(8,128)(2,1)} %copy-done.2), custom_call_target="tpu_custom_call" | custom-call | flops 22548578304 | bytes 4980736 | tf_op jit(solution)/shard_map/attend/pallas_call | solution.py:192
  190.1 0.0 collective-permute-done.refs_2_
  190.1 61.6 %attend.3 = bf16[3072,128]{1,0:T(8,128)(2,1)} custom-call(f32[2]{0:T(128)} %pad_maximum_fusion.1.refs_0_, bf16[3072,128]{1,0:T(8,128)(2,1)} %bitcast.14, bf16[4,896,256]{2,1,0:T(8,128)(2,1)} %collective-permute-done.refs_2_, f32[2,3072,128]{2,1,0:T(8,128)} %get-tuple-element.11.refs_3_, f32[2,3072,128]{2,1,0:T(8,128)} %get-tuple-element.12.refs_4_, ...), custom_call_target="tpu_custom_call" | custom-call | flops 22548578304 | bytes 4980736 | tf_op jit(solution)/shard_map/attend/pallas_call | solution.py:192
  251.6 3.6 %all-to-all-start.2 = ((bf16[16,192,128]{2,1,0:T(8,128)(2,1)}), bf16[16,192,128]{2,1,0:T(8,128)(2,1)S(1)}, u32[]{:S(2)}, u32[]{:S(2)}) async-start(bf16[16,192,128]{2,1,0:T(8,128)(2,1)} %bitcast.15), calls=%async_computation.2 | async-start | bytes 1572864 | tf_op jit(solution)/shard_map/all_to_all | solution.py:301
  255.3 0.1 reshape.59
  255.3 0.6 slice_bitcast_fusion.gate_ref
  255.9 18.0 %all-to-all-done.2.recv_ref = bf16[16,192,128]{2,1,0:T(8,128)(2,1)S(1)} async-done(((bf16[16,192,128]{2,1,0:T(8,128)(2,1)}), bf16[16,192,128]{2,1,0:T(8,128)(2,1)S(1)}, u32[]{:S(2)}, u32[]{:S(2)}) %all-to-all-start.2) | async-done | bytes 786464 | tf_op jit(solution)/shard_map/all_to_all | solution.py:301
  273.9 1.0 copy-done.1
  274.9 6.6 %finish.1 = bf16[192,2048]{1,0:T(8,128)(2,1)} custom-call(bf16[16,192,128]{2,1,0:T(8,128)(2,1)} %copy-done.1, bf16[2048,2048]{1,0:T(8,128)(2,1)} %all-gather.7.cloned.1.call-done.w_ref, bf16[192,2048]{1,0:T(8,128)(2,1)} %lat_ref.1, f32[1,2048]{1,0:T(1,128)} %slice_bitcast_fusion.gate_ref), custom_call_target="tpu_custom_call" | custom-call | flops 1610612736 | bytes 8388608 | tf_op jit(solution)/shard_map/finish/pallas_call | solution.py:225
  (21 shorter events, 0.1 us)
Async XLA Ops:
  6.5 1.5 copy-start
  6.5 2.3 copy-start.4
  6.5 3.2 %copy-start.5 = (bf16[256,512]{1,0:T(8,128)(2,1)S(1)}, bf16[256,512]{1,0:T(8,128)(2,1)}, u32[]{:S(2)}) copy-start(bf16[256,512]{1,0:T(8,128)(2,1)} %param.18) | copy-start | bytes 786436
  6.5 50.2 %all-gather.5.cloned.1.call-start = ((), (), s32[]{:S(2)}) async-start(), calls=%async_computation.3 | async-start | bytes 3932160 | tf_op jit(solution)/shard_map/all_gather | solution.py:283
  7.3 48.8 %copy-start.6 = (f32[2048]{0:T(1024)S(1)}, f32[2048]{0:T(1024)}, u32[]{:S(2)}) copy-start(f32[2048]{0:T(1024)} %param.17) | copy-start | bytes 24580
  7.3 266.6 %all-gather.7.cloned.1.call-start = ((), (), s32[]{:S(2)}) async-start(), calls=%async_computation.4 | async-start | bytes 10485760 | tf_op jit(solution)/shard_map/all_gather | solution.py:284
  69.7 50.8 %copy-start.7 = (f32[4]{0:T(128)S(1)}, f32[4]{0:T(128)}, u32[]{:S(2)}) copy-start(f32[4]{0:T(128)} %param.26) | copy-start | bytes 52
  69.7 51.4 %copy-start.8 = (f32[4]{0:T(128)S(1)}, f32[4]{0:T(128)}, u32[]{:S(2)}) copy-start(f32[4]{0:T(128)} %param.25) | copy-start | bytes 52
  116.8 23.4 %copy-start.2 = (bf16[4,896,256]{2,1,0:T(8,128)(2,1)}, bf16[4,896,256]{2,1,0:T(8,128)(2,1)S(1)}, u32[]{:S(2)}) copy-start(bf16[4,896,256]{2,1,0:T(8,128)(2,1)S(1)} %all_to_all.15.refs_2_) | copy-start | bytes 5505028
  116.8 23.4 %all-to-all-start = ((bf16[4,768,128]{2,1,0:T(8,128)(2,1)}), bf16[4,768,128]{2,1,0:T(8,128)(2,1)S(1)}, u32[]{:S(2)}, u32[]{:S(2)}) async-start(bf16[4,768,128]{2,1,0:T(8,128)(2,1)} %get-tuple-element.9), calls=%async_computation | async-start | bytes 1572864 | tf_op jit(solution)/shard_map/all_to_all | solution.py:291
  123.7 66.4 %collective-permute-start = (bf16[4,896,256]{2,1,0:T(8,128)(2,1)S(1)}, bf16[4,896,256]{2,1,0:T(8,128)(2,1)}, u32[]{:S(2)}, u32[]{:S(2)}) collective-permute-start(bf16[4,896,256]{2,1,0:T(8,128)(2,1)S(1)} %all_to_all.15.refs_2_), channel_id=1, source_target_pairs={{0,4},{4,0},{1,5},{5,1},{2,6},{6,2},{3,7},{7,3},{8,12},{12,8},{9,1... | collective-permute-start | bytes 5505032 | tf_op jit(solution)/shard_map/ppermute | solution.py:288
  140.2 0.9 copy-start.3
  251.6 22.3 %all-to-all-start.2 = ((bf16[16,192,128]{2,1,0:T(8,128)(2,1)}), bf16[16,192,128]{2,1,0:T(8,128)(2,1)S(1)}, u32[]{:S(2)}, u32[]{:S(2)}) async-start(bf16[16,192,128]{2,1,0:T(8,128)(2,1)} %bitcast.15), calls=%async_computation.2 | async-start | bytes 1572864 | tf_op jit(solution)/shard_map/all_to_all | solution.py:301
  273.9 1.0 copy-start.1
Sparse Core Ops, SparseCore 0:
  8.9 34.2 all-gather.4
  44.8 58.3 all-gather.6
